TPU v7x, 32 devices: a whole 2x2x4 slice. The times are simulated.
32 devices in a mesh: ep: 8 (over z, y), tp: 4 (over x, core).
Axes of the slice: x: 2, y: 2, z: 4, core: 2. Of those that a mesh axis runs over, the one named last changes fastest.
Arguments:
- tokens: bfloat16 [16, 2048], P('ep'), may hold values from -6 to 6
- state_c: float32 [16, 8, 128, 256], P('ep', 'tp'), may hold values from -0.8 to 0.8
- state_n: float32 [16, 8, 128], P('ep', 'tp'), may hold values from -0.8 to 0.8
- state_m: float32 [16, 8], P('ep', 'tp'), may hold values from -2 to 2
- mix_gain: float32 [2048], replicated, may hold values from 0.1 to 1.9
- w_query: bfloat16 [2048, 1024], P('ep', 'tp'), may hold values from -0.125 to 0.125
- w_key: bfloat16 [2048, 1024], P('ep', 'tp'), may hold values from -0.125 to 0.125
- w_value: bfloat16 [2048, 2048], P('ep', 'tp'), may hold values from -0.125 to 0.125
- w_input_gate: bfloat16 [2048, 8], replicated, may hold values from -0.125 to 0.125
- w_forget_gate: bfloat16 [2048, 8], replicated, may hold values from -0.125 to 0.125
- forget_bias: float32 [8], replicated, may hold values from -1 to 4
- w_output: bfloat16 [2048, 2048], P('tp', 'ep'), may hold values from -0.125 to 0.125
- moe_gain: float32 [2048], replicated, may hold values from 0.1 to 1.9
- w_group: bfloat16 [2048, 4], replicated, may hold values from -0.25 to 0.25
- expert_ids: int32 [16, 2], P('ep'), may hold values from 0 to 7, all different within a row; in each aligned block of 2 rows (0 to 1, 2 to 3, ...) at most 1 rows name the same one
- expert_weight: float32 [16, 2], P('ep'), may hold values from 0.1 to 1
- w_exp_gate: bfloat16 [8, 2048, 512], P('ep', None, 'tp'), may hold values from -0.125 to 0.125
- w_exp_up: bfloat16 [8, 2048, 512], P('ep', None, 'tp'), may hold values from -0.25 to 0.25
- w_exp_down: bfloat16 [8, 512, 2048], P('ep', 'tp'), may hold values from -1 to 1
- w_dense: bfloat16 [2048, 2048], P('ep', 'tp'), may hold values from -0.125 to 0.125
- w_dense_gate: bfloat16 [2048], replicated, may hold values from -0.125 to 0.125
Outputs:
- mixed: bfloat16 [16, 2048], P('ep', 'tp')
- new_c: float32 [16, 8, 128, 256], P('ep', 'tp')
- new_n: float32 [16, 8, 128], P('ep', 'tp')
- new_m: float32 [16, 8], P('ep', 'tp')
Inputs may be any that keep to these rules, and one draw needn't show every extreme that they name: `expert_ids`: each row names 2 different experts. In each aligned block of 2 rows (the rows of one index of ep) no expert is named by more than 1 row, a bound that some block reaches. Every expert is named by some row.
All inputs are finite; a program needn't handle non-finite values.
Results may differ from a plain program's by a relative error of at most 0.025.
Values may be sent and summed in bfloat16 or wider, within the bound.
No kernel may reach another device: no remote copies, remote signals or barrier semaphores. Data moves between devices by JAX's collectives and lax.ppermute only.
A program may use at most 64 MiB of HBM per device.

v0:
```python
import jax
import jax.numpy as jnp
from jax import lax
from jax.sharding import PartitionSpec as P

CAP = 1


eps = 1e-06


def rms_norm(values, gain):
    widened = values.astype(jnp.float32)
    inverse = lax.rsqrt(jnp.mean(widened * widened, axis=-1, keepdims=True) + eps)
    return (widened * inverse * gain).astype(jnp.bfloat16)


def rounded(values):
    return lax.optimization_barrier(values.astype(jnp.bfloat16)).astype(jnp.float32)


def memory_step(query_rows, key_rows, value_rows, in_gate, forget, state_c, state_n, state_m):
    seq_count, head_count = state_m.shape
    q_heads = query_rows.reshape(seq_count, head_count, -1)
    k_heads = key_rows.reshape(seq_count, head_count, -1) * q_heads.shape[-1] ** (-0.5)
    v_heads = value_rows.reshape(seq_count, head_count, -1)
    new_m = jnp.maximum(forget + state_m, in_gate)
    decay = jnp.exp(forget + state_m - new_m)
    inflow = jnp.exp(in_gate - new_m)
    new_c = (
        decay[..., None, None] * state_c
        + (inflow[..., None] * k_heads)[..., :, None] * v_heads[..., None, :]
    )
    new_n = decay[..., None] * state_n + inflow[..., None] * k_heads
    numer = jnp.einsum("shd,shde->she", q_heads, new_c, precision=lax.Precision.HIGHEST)
    denom = jnp.maximum(jnp.abs(jnp.sum(q_heads * new_n, axis=-1)), 1.0)
    heads = (numer / denom[..., None]).astype(jnp.bfloat16).reshape(seq_count, -1)
    return (heads, new_c, new_n, new_m)


def per_device(
    tokens,
    state_c,
    state_n,
    state_m,
    mix_gain,
    w_query,
    w_key,
    w_value,
    w_input_gate,
    w_forget_gate,
    forget_bias,
    w_output,
    moe_gain,
    w_group,
    expert_ids,
    expert_weight,
    w_exp_gate,
    w_exp_up,
    w_exp_down,
    w_dense,
    w_dense_gate,
):
    seq_count = tokens.shape[0]
    width = tokens.shape[1]
    tp_count = lax.axis_size("tp")
    ep_count = lax.axis_size("ep")
    tp_rank = lax.axis_index("tp")
    head_count = state_m.shape[1]
    qk_cols = w_query.shape[1]
    share = width // tp_count
    normed = rms_norm(tokens, mix_gain)
    spread_cols = lax.all_to_all(normed, "ep", split_axis=1, concat_axis=0, tiled=True)
    joined = jnp.concatenate([w_query, w_key, w_value], axis=1)
    token_rows = spread_cols
    summed = lax.psum_scatter(
        jnp.dot(token_rows, joined, preferred_element_type=jnp.float32),
        "ep",
        scatter_dimension=0,
        tiled=True,
    )
    query_sum = summed[:, :qk_cols]
    key_sum = summed[:, qk_cols : 2 * qk_cols]
    value_sum = summed[:, 2 * qk_cols :]
    query_rows = rounded(query_sum)
    key_rows = rounded(key_sum)
    value_rows = rounded(value_sum)
    gate_all = jnp.dot(normed, w_input_gate, preferred_element_type=jnp.float32)
    forget_all = jax.nn.log_sigmoid(
        jnp.dot(normed, w_forget_gate, preferred_element_type=jnp.float32) + forget_bias
    )
    in_gate = lax.dynamic_slice_in_dim(gate_all, tp_rank * head_count, head_count, 1)
    forget = lax.dynamic_slice_in_dim(forget_all, tp_rank * head_count, head_count, 1)
    heads, new_c, new_n, new_m = memory_step(
        query_rows, key_rows, value_rows, in_gate, forget, state_c, state_n, state_m
    )
    row_parts = jnp.dot(
        lax.all_gather(heads, "ep", axis=0, tiled=True),
        w_output,
        preferred_element_type=jnp.float32,
    ).astype(jnp.bfloat16)
    partial_value = lax.all_to_all(row_parts, "ep", split_axis=0, concat_axis=1, tiled=True).astype(
        jnp.float32
    )
    mixer_sum = lax.psum(partial_value.astype(jnp.bfloat16), "tp").astype(jnp.float32)
    residual = (tokens.astype(jnp.float32) + mixer_sum).astype(jnp.bfloat16)
    normed2 = rms_norm(residual, moe_gain)
    group_count = w_group.shape[1]
    group_prob = jax.nn.softmax(
        jnp.dot(normed2, w_group, preferred_element_type=jnp.float32), axis=-1
    )
    experts_here = w_exp_gate.shape[0]
    expert_count = experts_here * ep_count
    per_group = expert_count // group_count
    top_count = expert_ids.shape[1]
    member = (expert_ids // per_group)[..., None] == jnp.arange(group_count, dtype=jnp.int32)[
        None, None, :
    ]
    picked = jnp.sum(jnp.where(member, group_prob[:, None, :], 0.0), axis=-1)
    route = picked * expert_weight / jnp.sum(expert_weight, axis=1, keepdims=True)
    flat_ids = expert_ids.reshape(-1)
    assigned = flat_ids[:, None] == jnp.arange(expert_count, dtype=jnp.int32)[None, :]
    ranks = jnp.cumsum(assigned.astype(jnp.int32), axis=0) - 1
    own_rank = jnp.sum(jnp.where(assigned, ranks, 0), axis=1)
    slot_index = flat_ids * CAP + own_rank
    placing = (
        jnp.arange(expert_count * CAP, dtype=jnp.int32)[:, None] == slot_index[None, :]
    ).astype(jnp.bfloat16)
    repeated = jnp.repeat(normed2, top_count, axis=0)
    outgoing = jnp.dot(placing, repeated, preferred_element_type=jnp.float32).astype(jnp.bfloat16)
    outgoing = outgoing.reshape(expert_count, CAP, width)
    arrived = lax.all_to_all(outgoing, "ep", split_axis=0, concat_axis=0, tiled=True)
    slots = arrived.shape[1]
    grid_rows = arrived.reshape(ep_count, experts_here, slots, width)
    gate_act = jnp.einsum(
        "sxnd,xdf->sxnf", grid_rows, w_exp_gate, preferred_element_type=jnp.float32
    )
    up_act = jnp.einsum("sxnd,xdf->sxnf", grid_rows, w_exp_up, preferred_element_type=jnp.float32)
    hidden = (jax.nn.silu(gate_act) * up_act).astype(jnp.bfloat16)
    down_part = jnp.einsum("sxnf,xfd->sxnd", hidden, w_exp_down, preferred_element_type=jnp.float32)
    reduced = lax.psum_scatter(
        down_part.astype(jnp.bfloat16), "tp", scatter_dimension=3, tiled=True
    )
    returned = lax.all_to_all(
        reduced.reshape(expert_count, slots, share), "ep", split_axis=0, concat_axis=0, tiled=True
    )
    picked_rows = jnp.einsum(
        "ca,cd->ad",
        placing,
        returned.reshape(expert_count * CAP, share),
        preferred_element_type=jnp.float32,
    )
    moe = jnp.sum(route[..., None] * picked_rows.reshape(seq_count, top_count, share), axis=1)
    dense_cols = lax.all_to_all(normed2, "ep", split_axis=1, concat_axis=0, tiled=True)
    token_rows = dense_cols
    dense_raw = lax.psum_scatter(
        jnp.dot(token_rows, w_dense, preferred_element_type=jnp.float32),
        "ep",
        scatter_dimension=0,
        tiled=True,
    )
    dense_gate = jax.nn.sigmoid(jnp.dot(normed2, w_dense_gate, preferred_element_type=jnp.float32))
    own_cols = lax.dynamic_slice_in_dim(residual, tp_rank * share, share, 1).astype(jnp.float32)
    mixed = (own_cols + moe + dense_gate[:, None] * dense_raw).astype(jnp.bfloat16)
    return (mixed, new_c, new_n, new_m)


def solution(mesh):
    placed = (
        P("ep", None),
        P("ep", "tp", None, None),
        P("ep", "tp", None),
        P("ep", "tp"),
        P(),
        P("ep", "tp"),
        P("ep", "tp"),
        P("ep", "tp"),
        P(),
        P(),
        P(),
        P("tp", "ep"),
        P(),
        P(),
        P("ep", None),
        P("ep", None),
        P("ep", None, "tp"),
        P("ep", None, "tp"),
        P("ep", "tp", None),
        P("ep", "tp"),
        P(),
    )
    return jax.shard_map(
        per_device,
        mesh=mesh,
        in_specs=placed,
        out_specs=(P("ep", "tp"), P("ep", "tp", None, None), P("ep", "tp", None), P("ep", "tp")),
        check_vma=False,
    )
```

profile of v0, /device:TPU:0, one launch (start us, length us, event | category | flops | bytes accessed | tf_op | source)
XLA Modules:
  0.0 200.7 jit_solution(5687725438537635701)
XLA Ops:
  7.2 0.9 fusion.27
  8.1 1.4 fusion.29
  9.5 7.4 %all-to-all-start = ((bf16[2,8,256]{2,0,1:T(2,128)(2,1)}), bf16[2,8,256]{2,0,1:T(2,128)(2,1)S(1)}, u32[]{:S(2)}, u32[]{:S(2)}) async-start(bf16[2,8,256]{2,0,1:T(2,128)(2,1)} %bitcast), calls=%async_computation | async-start | bytes 16384 | tf_op jit(solution)/shard_map/all_to_all | solution.py:73
  17.7 0.8 fusion.58
  18.5 0.9 fusion.48
  22.3 1.1 all-to-all-done
  23.5 1.2 fusion.11
  24.7 36.9 %all-reduce = bf16[16,1024]{1,0:T(8,128)(2,1)S(1)} all-reduce(f32[16,1024]{1,0:T(8,128)S(1)} %fusion.11), channel_id=2, replica_groups=mesh['ep'=8,'tp'=4] {'ep'}, use_global_device_ids=true, to_apply=%region_1.0.clone | all-reduce | flops 16384 | bytes 98304
  64.2 26.2 %all-gather = bf16[8,2,512]{2,1,0:T(2,128)(2,1)S(1)} all-gather(bf16[1,2,512]{2,1,0:T(2,128)(2,1)S(1)} %reshape.161), channel_id=1, replica_groups=mesh['ep'=8,'tp'=4] {'ep'}, dimensions={0}, use_global_device_ids=true | all-gather | bytes 18432 | tf_op jit(solution)/shard_map/all_gather | solution.py:98
  91.3 3.3 %all-to-all-start.1 = ((bf16[8,2,256]{2,1,0:T(2,128)(2,1)}), bf16[8,2,256]{2,1,0:T(2,128)(2,1)S(1)}, u32[]{:S(2)}, u32[]{:S(2)}) async-start(bf16[8,2,256]{2,1,0:T(2,128)(2,1)} %all_to_all.52), calls=%async_computation.1 | async-start | bytes 16384 | tf_op jit(solution)/shard_map/all_to_all | solution.py:102
  94.8 6.2 %all-to-all-done.1 = bf16[8,2,256]{2,1,0:T(2,128)(2,1)S(1)} async-done(((bf16[8,2,256]{2,1,0:T(2,128)(2,1)}), bf16[8,2,256]{2,1,0:T(2,128)(2,1)S(1)}, u32[]{:S(2)}, u32[]{:S(2)}) %all-to-all-start.1) | async-done | bytes 8224 | tf_op jit(solution)/shard_map/all_to_all | solution.py:102
  101.1 5.7 %psum.7 = bf16[2,2048]{1,0:T(2,128)(2,1)S(1)} all-reduce(bf16[2,2048]{1,0:T(2,128)(2,1)S(1)} %bitcast.93), channel_id=1, replica_groups=mesh['ep'=8,'tp'=4] {'tp'}, use_global_device_ids=true, to_apply=%region_3.4 | all-reduce | flops 4096 | bytes 16384 | tf_op jit(solution)/shard_map/psum | solution.py:105
  107.6 0.9 fusion.57
  108.8 0.7 broadcast_in_dim.16
  109.6 3.4 %all-to-all-start.4 = ((bf16[2,8,256]{2,0,1:T(2,128)(2,1)}), bf16[2,8,256]{2,0,1:T(2,128)(2,1)S(1)}, u32[]{:S(2)}, u32[]{:S(2)}) async-start(bf16[2,8,256]{2,0,1:T(2,128)(2,1)} %bitcast.23), calls=%async_computation.5 | async-start | bytes 16384 | tf_op jit(solution)/shard_map/all_to_all | solution.py:154
  113.0 0.9 fusion.10
  116.0 3.5 %all-to-all-done.4 = bf16[2,8,256]{2,0,1:T(2,128)(2,1)S(1)} async-done(((bf16[2,8,256]{2,0,1:T(2,128)(2,1)}), bf16[2,8,256]{2,0,1:T(2,128)(2,1)S(1)}, u32[]{:S(2)}, u32[]{:S(2)}) %all-to-all-start.4) | async-done | bytes 8224 | tf_op jit(solution)/shard_map/all_to_all | solution.py:154
  119.5 3.3 %all-to-all-start.2 = ((bf16[8,2,1024]{2,1,0:T(2,128)(2,1)}), bf16[8,2,1024]{2,1,0:T(2,128)(2,1)S(1)}, u32[]{:S(2)}, u32[]{:S(2)}) async-start(bf16[8,2,1024]{2,1,0:T(2,128)(2,1)} %reshape.175), calls=%async_computation.2 | async-start | bytes 65536 | tf_op jit(solution)/shard_map/all_to_all | solution.py:132
  123.0 6.5 %all-to-all-done.2 = bf16[8,2,1024]{2,1,0:T(2,128)(2,1)S(1)} async-done(((bf16[8,2,1024]{2,1,0:T(2,128)(2,1)}), bf16[8,2,1024]{2,1,0:T(2,128)(2,1)S(1)}, u32[]{:S(2)}, u32[]{:S(2)}) %all-to-all-start.2) | async-done | bytes 32800 | tf_op jit(solution)/shard_map/all_to_all | solution.py:132
  129.7 1.0 fusion.1
  130.8 17.1 %reduce-scatter.2.cloned.1.call-done = bf16[8,1,1,512]{3,0,2,1:T(8,128)(2,1)} async-done(((bf16[8,1,1,2048]{3,0,2,1:T(8,128)(2,1)}), bf16[8,1,1,512]{3,0,2,1:T(8,128)(2,1)}) %reduce-scatter.2.cloned.1.call-update) | async-done | bytes 8208 | tf_op jit(solution)/shard_map/reduce_scatter | solution.py:141
  148.0 1.3 reduce.1
  149.9 5.5 %all-to-all-start.3 = ((bf16[8,2,256]{2,1,0:T(2,128)(2,1)}), bf16[8,2,256]{2,1,0:T(2,128)(2,1)S(1)}, u32[]{:S(2)}, u32[]{:S(2)}) async-start(bf16[8,2,256]{2,1,0:T(2,128)(2,1)} %reshape.177), calls=%async_computation.4 | async-start | bytes 16384 | tf_op jit(solution)/shard_map/all_to_all | solution.py:144
  155.4 37.6 %all-reduce.1 = f32[16,512]{1,0:T(8,128)S(1)} all-reduce(f32[16,512]{1,0:T(8,128)S(1)} %fusion.60), channel_id=4, replica_groups=mesh['ep'=8,'tp'=4] {'ep'}, use_global_device_ids=true, to_apply=%region_13.14.clone | all-reduce | flops 8192 | bytes 65536
  (97 shorter events, 11.6 us)
Async XLA Ops:
  7.2 122.5 %copy-start = (bf16[1,128,2048]{2,1,0:T(8,128)(2,1)S(1)}, bf16[1,128,2048]{2,1,0:T(8,128)(2,1)}, u32[]{:S(2)}) copy-start(bf16[1,128,2048]{2,1,0:T(8,128)(2,1)} %param.39) | copy-start | bytes 1572868
  7.2 0.9 copy-start.7
  7.2 10.5 %copy-start.17 = (bf16[2048,8]{0,1:T(8,128)(2,1)S(1)}, bf16[2048,8]{0,1:T(8,128)(2,1)}, u32[]{:S(2)}) copy-start(bf16[2048,8]{0,1:T(8,128)(2,1)} %param.29) | copy-start | bytes 98308
  9.5 9.0 %copy-start.19 = (f32[8]{0:T(128)S(1)}, f32[8]{0:T(128)}, u32[]{:S(2)}) copy-start(f32[8]{0:T(128)} %param.31) | copy-start | bytes 100
  9.5 14.0 %all-to-all-start = ((bf16[2,8,256]{2,0,1:T(2,128)(2,1)}), bf16[2,8,256]{2,0,1:T(2,128)(2,1)S(1)}, u32[]{:S(2)}, u32[]{:S(2)}) async-start(bf16[2,8,256]{2,0,1:T(2,128)(2,1)} %bitcast), calls=%async_computation | async-start | bytes 16384 | tf_op jit(solution)/shard_map/all_to_all | solution.py:73
  16.9 6.5 %copy-start.16 = (bf16[256,256]{1,0:T(8,128)(2,1)S(1)}, bf16[256,256]{1,0:T(8,128)(2,1)}, u32[]{:S(2)}) copy-start(bf16[256,256]{1,0:T(8,128)(2,1)} %param.27) | copy-start | bytes 393220
  18.5 0.9 copy-start.15
  23.5 40.1 %copy-start.2 = (f32[2,2,128,256]{3,2,1,0:T(8,128)S(1)}, f32[2,2,128,256]{3,2,1,0:T(8,128)}, u32[]{:S(2)}) copy-start(f32[2,2,128,256]{3,2,1,0:T(8,128)} %param.22) | copy-start | bytes 1572868
  62.2 0.7 copy-start.13
  62.2 0.7 slice-start
  63.8 44.8 %copy-start.1 = (f32[2,2,128,256]{3,2,1,0:T(8,128)}, f32[2,2,128,256]{3,2,1,0:T(8,128)S(1)}, u32[]{:S(2)}) copy-start(f32[2,2,128,256]{3,2,1,0:T(8,128)S(1)} %multiply_add_fusion) | copy-start | bytes 1572868
  63.8 26.7 %copy-start.6 = (bf16[512,256]{1,0:T(8,128)(2,1)S(1)}, bf16[512,256]{1,0:T(8,128)(2,1)}, u32[]{:S(2)}) copy-start(bf16[512,256]{1,0:T(8,128)(2,1)} %param.32) | copy-start | bytes 786436
  63.8 30.9 %copy-start.10 = (bf16[2048]{0:T(1024)(128)(2,1)S(1)}, bf16[2048]{0:T(1024)(128)(2,1)}, u32[]{:S(2)}) copy-start(bf16[2048]{0:T(1024)(128)(2,1)} %param.41) | copy-start | bytes 12292
  63.8 30.9 %copy-start.11 = (f32[2,2]{1,0:T(2,128)S(1)}, f32[2,2]{1,0:T(2,128)}, u32[]{:S(2)}) copy-start(f32[2,2]{1,0:T(2,128)} %param.36) | copy-start | bytes 52
  63.8 43.1 %copy-start.9 = (f32[2048]{0:T(1024)S(1)}, f32[2048]{0:T(1024)}, u32[]{:S(2)}) copy-start(f32[2048]{0:T(1024)} %param.33) | copy-start | bytes 24580
  63.8 43.8 %copy-start.18 = (bf16[2048,4]{0,1:T(4,128)(2,1)S(1)}, bf16[2048,4]{0,1:T(4,128)(2,1)}, u32[]{:S(2)}) copy-start(bf16[2048,4]{0,1:T(4,128)(2,1)} %param.34) | copy-start | bytes 49156
  64.2 65.3 %copy-start.3 = (bf16[1,2048,128]{2,1,0:T(8,128)(2,1)S(1)}, bf16[1,2048,128]{2,1,0:T(8,128)(2,1)}, u32[]{:S(2)}) copy-start(bf16[1,2048,128]{2,1,0:T(8,128)(2,1)} %param.37) | copy-start | bytes 1572868
  91.3 9.8 %all-to-all-start.1 = ((bf16[8,2,256]{2,1,0:T(2,128)(2,1)}), bf16[8,2,256]{2,1,0:T(2,128)(2,1)S(1)}, u32[]{:S(2)}, u32[]{:S(2)}) async-start(bf16[8,2,256]{2,1,0:T(2,128)(2,1)} %all_to_all.52), calls=%async_computation.1 | async-start | bytes 16384 | tf_op jit(solution)/shard_map/all_to_all | solution.py:102
  109.6 20.1 %copy-start.4 = (bf16[1,2048,128]{2,1,0:T(8,128)(2,1)S(1)}, bf16[1,2048,128]{2,1,0:T(8,128)(2,1)}, u32[]{:S(2)}) copy-start(bf16[1,2048,128]{2,1,0:T(8,128)(2,1)} %param.38) | copy-start | bytes 1572868
  109.6 9.9 %all-to-all-start.4 = ((bf16[2,8,256]{2,0,1:T(2,128)(2,1)}), bf16[2,8,256]{2,0,1:T(2,128)(2,1)S(1)}, u32[]{:S(2)}, u32[]{:S(2)}) async-start(bf16[2,8,256]{2,0,1:T(2,128)(2,1)} %bitcast.23), calls=%async_computation.5 | async-start | bytes 16384 | tf_op jit(solution)/shard_map/all_to_all | solution.py:154
  119.5 10.0 %all-to-all-start.2 = ((bf16[8,2,1024]{2,1,0:T(2,128)(2,1)}), bf16[8,2,1024]{2,1,0:T(2,128)(2,1)S(1)}, u32[]{:S(2)}, u32[]{:S(2)}) async-start(bf16[8,2,1024]{2,1,0:T(2,128)(2,1)} %reshape.175), calls=%async_computation.2 | async-start | bytes 65536 | tf_op jit(solution)/shard_map/all_to_all | solution.py:132
  122.8 25.1 %reduce-scatter.2.cloned.1.call-start = ((), (), s32[]{:S(2)}) async-start(), calls=%async_computation.6 | async-start | bytes 40960 | tf_op jit(solution)/shard_map/reduce_scatter | solution.py:141
  129.7 1.0 copy-start.5
  149.9 43.1 %all-to-all-start.3 = ((bf16[8,2,256]{2,1,0:T(2,128)(2,1)}), bf16[8,2,256]{2,1,0:T(2,128)(2,1)S(1)}, u32[]{:S(2)}, u32[]{:S(2)}) async-start(bf16[8,2,256]{2,1,0:T(2,128)(2,1)} %reshape.177), calls=%async_computation.4 | async-start | bytes 16384 | tf_op jit(solution)/shard_map/all_to_all | solution.py:144
  (4 other events, 2.5 us)
Sparse Core Ops, SparseCore 0:
  130.8 17.1 reduce-scatter.1
where the time goes:
time: 202 us; the launch traced here: 201 us
  blocking collectives  106 us (52%)
  waiting for transfers between devices  34.5 us (17%)
  starting transfers between devices  23.1 us (11%)
  between operations  15 us (7%)
  other arithmetic  7.76 us (4%)
  local copies, waits for them, and re-layouts  7.08 us (4%)
  matrix products  6.76 us (3%)
    unnamed x2, blocking collectives  74.5 us
    all_gather x1, blocking collectives, per_device(): lax.all_gather(heads, 'ep', axis=0, tiled=True)  26.2 us
    reduce_scatter x1, waiting for transfers between devices, per_device(): lax.psum_scatter(down_part.astype(jnp.bfloat16), 'tp', scatter_dimension=...  17.1 us
    all_to_all x1, starting transfers between devices, per_device(): lax.all_to_all(normed, 'ep', split_axis=1, concat_axis=0, tiled=True)  7.44 us
    all_to_all x1, waiting for transfers between devices, per_device(): lax.all_to_all(outgoing, 'ep', split_axis=0, concat_axis=0, tiled=True)  6.49 us
    all_to_all x1, waiting for transfers between devices, per_device(): lax.all_to_all(row_parts, 'ep', split_axis=0, concat_axis=1, tiled=True)  6.22 us
    psum x1, blocking collectives, per_device(): lax.psum(partial_value.astype(jnp.bfloat16), 'tp').astype(jnp.float32)  5.74 us
    all_to_all x1, starting transfers between devices, per_device(): lax.all_to_all(reduced.reshape(expert_count, slots, share), 'ep', split_a...  5.51 us
  transfers between devices with their start and end apart: 6, of which 5 were waited for; matrix products, arithmetic and copies ran while one was open for 3% of the time, Pallas kernels for 0%

commit v1 on v0

v1 whole, which is shorter than its diff:
```python
import jax
import jax.numpy as jnp
from jax import lax
from jax.sharding import PartitionSpec as P

eps = 1e-06
BOTH = ("ep", "tp")


def exchange(chunks, axes):
    return lax.all_to_all(chunks, axes, split_axis=0, concat_axis=0, tiled=True)


def rms_norm(values, gain):
    widened = values.astype(jnp.float32)
    inverse = lax.rsqrt(jnp.mean(widened * widened, axis=-1, keepdims=True) + eps)
    return (widened * inverse * gain).astype(jnp.bfloat16)


def per_device(
    tokens,
    state_c,
    state_n,
    state_m,
    mix_gain,
    w_query,
    w_key,
    w_value,
    w_input_gate,
    w_forget_gate,
    forget_bias,
    w_output,
    moe_gain,
    w_group,
    expert_ids,
    expert_weight,
    w_exp_gate,
    w_exp_up,
    w_exp_down,
    w_dense,
    w_dense_gate,
):
    f32, bf16 = jnp.float32, jnp.bfloat16
    own, width = tokens.shape
    tp_count = lax.axis_size("tp")
    ep_count = lax.axis_size("ep")
    tp_rank = lax.axis_index("tp")
    ep_rank = lax.axis_index("ep")
    seqs = own * ep_count
    head_count = state_m.shape[1]
    rows = w_query.shape[0]
    qk_cols = w_query.shape[1]
    share = width // tp_count
    cols = w_output.shape[1]
    experts_here = w_exp_gate.shape[0]
    expert_count = experts_here * ep_count

    spread = exchange(tokens.reshape(own, ep_count, rows).transpose(1, 0, 2), "ep")
    spread = spread.reshape(seqs, rows)
    gain_rows = lax.dynamic_slice_in_dim(mix_gain, ep_rank * rows, rows)
    scaled = (spread.astype(f32) * gain_rows).astype(bf16)
    sums = [jnp.dot(scaled, w, preferred_element_type=f32) for w in (w_query, w_key, w_value)]
    expert_of = jnp.arange(expert_count, dtype=jnp.int32)
    shares = expert_weight / jnp.sum(expert_weight, axis=1, keepdims=True)
    picks = jnp.sum(
        jnp.where(expert_ids[None, :, :] == expert_of[:, None, None], shares[None], 0.0), axis=2
    )
    picks = picks.reshape(ep_count, experts_here, own).transpose(0, 2, 1)
    picks = jnp.pad(picks, ((0, 0), (0, 0), (0, -experts_here % 128))).reshape(seqs, -1)
    parts = exchange(jnp.concatenate(sums + [picks], axis=1).reshape(ep_count, own, -1), "ep")
    wide = tokens.astype(f32)
    inverse = lax.rsqrt(jnp.mean(wide * wide, axis=-1, keepdims=True) + eps)
    normed = (wide * inverse * mix_gain).astype(bf16)
    packed = 2 * qk_cols + w_value.shape[1]
    coef = parts[:, :, packed : packed + experts_here].reshape(seqs, experts_here)
    qkv = (jnp.sum(parts[:, :, :packed], axis=0) * inverse).astype(bf16).astype(f32)
    gate_all = jnp.dot(normed, w_input_gate, preferred_element_type=f32)
    forget_all = jax.nn.log_sigmoid(
        jnp.dot(normed, w_forget_gate, preferred_element_type=f32) + forget_bias
    )
    in_gate = lax.dynamic_slice_in_dim(gate_all, tp_rank * head_count, head_count, 1)
    forget = lax.dynamic_slice_in_dim(forget_all, tp_rank * head_count, head_count, 1)
    q_heads = qkv[:, :qk_cols].reshape(own, head_count, -1)
    k_heads = qkv[:, qk_cols : 2 * qk_cols].reshape(own, head_count, -1)
    k_heads = k_heads * q_heads.shape[-1] ** (-0.5)
    v_heads = qkv[:, 2 * qk_cols :].reshape(own, head_count, -1)
    new_m = jnp.maximum(forget + state_m, in_gate)
    decay = jnp.exp(forget + state_m - new_m)
    inflow = jnp.exp(in_gate - new_m)
    new_c = (
        decay[..., None, None] * state_c
        + (inflow[..., None] * k_heads)[..., :, None] * v_heads[..., None, :]
    )
    new_n = decay[..., None] * state_n + inflow[..., None] * k_heads
    recalled = jnp.sum(q_heads[..., None] * state_c, axis=2)
    match = jnp.sum(q_heads * k_heads, axis=-1)
    numer = decay[..., None] * recalled + (inflow * match)[..., None] * v_heads
    denom = jnp.maximum(jnp.abs(jnp.sum(q_heads * new_n, axis=-1)), 1.0)
    heads = (numer / denom[..., None]).astype(bf16).reshape(own, -1)
    heads_all = exchange(jnp.broadcast_to(heads[None], (ep_count,) + heads.shape), "ep")
    out_part = jnp.dot(heads_all.reshape(seqs, -1), w_output, preferred_element_type=f32)
    out_part = (out_part + spread.astype(f32) * (1.0 / tp_count)).astype(bf16)
    every = exchange(jnp.broadcast_to(out_part[None], (ep_count * tp_count,) + out_part.shape), BOTH)
    residual = jnp.sum(every.reshape(ep_count, tp_count, seqs, cols).astype(f32), axis=1)
    residual = residual.astype(bf16).transpose(1, 0, 2).reshape(seqs, width)
    normed2 = rms_norm(residual, moe_gain)
    group_count = w_group.shape[1]
    group_prob = jax.nn.softmax(jnp.dot(normed2, w_group, preferred_element_type=f32), axis=-1)
    group_of = (ep_rank * experts_here + jnp.arange(experts_here, dtype=jnp.int32)) // (
        expert_count // group_count
    )
    member = group_of[:, None] == jnp.arange(group_count, dtype=jnp.int32)[None, :]
    chance = jnp.sum(jnp.where(member[None], group_prob[:, None, :], 0.0), axis=-1)
    route = chance * coef
    total = jnp.zeros((seqs, width), f32)
    for x in range(experts_here):
        gate_act = jnp.dot(normed2, w_exp_gate[x], preferred_element_type=f32)
        up_act = jnp.dot(normed2, w_exp_up[x], preferred_element_type=f32)
        hidden = (jax.nn.silu(gate_act) * up_act).astype(bf16)
        total += route[:, x : x + 1] * jnp.dot(hidden, w_exp_down[x], preferred_element_type=f32)
    dense_gate = jax.nn.sigmoid(jnp.dot(normed2, w_dense_gate, preferred_element_type=f32))
    dense_in = lax.dynamic_slice_in_dim(normed2, ep_rank * rows, rows, 1)
    dense = dense_gate[:, None] * jnp.dot(dense_in, w_dense, preferred_element_type=f32)
    total = total.reshape(seqs, tp_count, share)
    mine = jnp.arange(tp_count, dtype=jnp.int32) == tp_rank
    total = (total + jnp.where(mine[None, :, None], dense[:, None, :], 0.0)).astype(bf16)
    total = total.reshape(ep_count, own, tp_count, share).transpose(0, 2, 1, 3)
    last = exchange(total.reshape(ep_count * tp_count, own, share), BOTH)
    own_rows = lax.dynamic_slice(residual, (ep_rank * own, tp_rank * share), (own, share))
    mixed = (own_rows.astype(f32) + jnp.sum(last.astype(f32), axis=0)).astype(bf16)
    return (mixed, new_c, new_n, new_m)


def solution(mesh):
    placed = (
        P("ep", None),
        P("ep", "tp", None, None),
        P("ep", "tp", None),
        P("ep", "tp"),
        P(),
        P("ep", "tp"),
        P("ep", "tp"),
        P("ep", "tp"),
        P(),
        P(),
        P(),
        P("tp", "ep"),
        P(),
        P(),
        P("ep", None),
        P("ep", None),
        P("ep", None, "tp"),
        P("ep", None, "tp"),
        P("ep", "tp", None),
        P("ep", "tp"),
        P(),
    )
    return jax.shard_map(
        per_device,
        mesh=mesh,
        in_specs=placed,
        out_specs=(P("ep", "tp"), P("ep", "tp", None, None), P("ep", "tp", None), P("ep", "tp")),
        check_vma=False,
    )
```

time: 202 us -> 70.7 us (0.35)
  blocking collectives: 106 us -> 0 us
  between operations: 15 us -> 0.95 us
  waiting for transfers between devices: 34.5 us -> 30.8 us
  matrix products: 6.76 us -> 3.27 us
    unnamed x2 -> x0, blocking collectives: 74.5 us -> none
    all_gather x1 -> x0, blocking collectives: 26.2 us -> none  [per_device(): lax.all_gather(heads, 'ep', axis=0, tiled=True)]
    reduce_scatter x1 -> x0, waiting for transfers between devices: 17.1 us -> none  [per_device(): lax.psum_scatter(down_part.astype(jnp.bfloat16), 'tp', scatter_dimension=...]
    all_to_all x5, waiting for transfers between devices: 17.3 us -> 30.8 us  [exchange(): return lax.all_to_all(chunks, axes, split_axis=0, concat_axis=0, tiled=True)]
    psum x1 -> x0, blocking collectives: 5.74 us -> none  [per_device(): lax.psum(partial_value.astype(jnp.bfloat16), 'tp').astype(jnp.float32)]
    dot_general x12 -> x11, matrix products: 6.76 us -> 3.27 us  [the longest x1 0.9 us: per_device(): jnp.dot(normed, w_forget_gate, preferred_element_type=f32) + forget_bias]
    unnamed x50 -> x40, local copies, waits for them, and re-layouts: 4.35 us -> 2.56 us
  transfers between devices with their start and end apart: 6 -> 5, of which waited for: 5 -> 5; matrix products, arithmetic and copies ran while one was open for 3% -> 9% of each run, Pallas kernels for 0% -> 0%
where the time goes in v1:
time: 70.7 us; the launch traced here: 69.8 us
  waiting for transfers between devices  30.8 us (44%)
  starting transfers between devices  21.5 us (30%)
  other arithmetic  6.71 us (9%)
  local copies, waits for them, and re-layouts  6.55 us (9%)
  matrix products  3.27 us (5%)
  between operations  0.95 us (1%)
    all_to_all x5, waiting for transfers between devices, exchange(): return lax.all_to_all(chunks, axes, split_axis=0, concat_axis=0, tiled=True)  30.8 us
    all_to_all x5, starting transfers between devices, exchange(): return lax.all_to_all(chunks, axes, split_axis=0, concat_axis=0, tiled=True)  21.5 us
    unnamed x40, local copies, waits for them, and re-layouts  2.56 us
  transfers between devices with their start and end apart: 5, of which 5 were waited for; matrix products, arithmetic and copies ran while one was open for 9% of the time, Pallas kernels for 0%

profile of v1, /device:TPU:0, one launch (start us, length us, event | category | flops | bytes accessed | tf_op | source)
XLA Modules:
  0.0 69.8 jit_solution(2563209829029870365)
XLA Ops:
  0.7 7.5 %all-to-all-start = ((bf16[8,2,256]{2,1,0:T(2,128)(2,1)}), bf16[8,2,256]{2,1,0:T(2,128)(2,1)S(1)}, u32[]{:S(2)}, u32[]{:S(2)}) async-start(bf16[8,2,256]{2,1,0:T(2,128)(2,1)} %bitcast.75), calls=%async_computation | async-start | bytes 16384 | tf_op jit(solution)/shard_map/all_to_all | solution.py:11
  8.2 0.9 %fusion.24 = f32[2]{0:T(128)S(1)} fusion(bf16[2,2048]{1,0:T(2,128)(2,1)} %param.21), kind=kLoop, calls=%fused_computation.44 | loop fusion | flops 12286 | bytes 8200 | tf_op jit(solution)/shard_map/reduce_sum | solution.py:72
  9.0 0.8 %reduce_sum.112 = f32[2]{0:T(128)S(1)} reduce(f32[2,2]{1,0:T(2,128)} %param.36, f32[]{:T(128)} %constant.27.clone.1), dimensions={1}, to_apply=%region_1.2 | reduce | flops 2 | bytes 28 | tf_op jit(solution)/shard_map/reduce_sum | solution.py:64
  9.8 0.7 %broadcast_divide_fusion = f32[2,2]{1,0:T(2,128)S(1)} fusion(f32[2,2]{1,0:T(2,128)} %param.36, f32[2]{0:T(128)S(1)} %reduce_sum.112), kind=kLoop, calls=%fused_computation.86 | loop fusion | flops 4 | bytes 40 | tf_op jit(solution)/shard_map/div | solution.py:64
  10.6 0.8 %fusion.26 = bf16[2,2048]{1,0:T(2,128)(2,1)S(1)} fusion(bf16[2,2048]{1,0:T(2,128)(2,1)} %param.21, f32[2]{0:T(128)S(1)} %add_rsqrt_fusion.1, f32[2048]{0:T(1024)} %param.25), kind=kLoop, calls=%fused_computation.46 | loop fusion | flops 16384 | bytes 24584 | tf_op jit(solution)/shard_map/convert_element_type | solution.py:73
  11.4 0.9 %fusion.50 = f32[2,8]{1,0:T(2,128)S(1)} fusion(bf16[2,2048]{1,0:T(2,128)(2,1)S(1)} %fusion.26, bf16[2048,8]{0,1:T(8,128)(2,1)} %param.29), kind=kOutput, calls=%fused_computation.92 | convolution fusion | flops 65536 | bytes 41024 | tf_op jit(solution)/shard_map/dot_general | solution.py:77
  12.3 0.9 %fusion.42 = f32[2,8]{1,0:T(2,128)S(1)} fusion(bf16[2,2048]{1,0:T(2,128)(2,1)S(1)} %fusion.26, bf16[2048,8]{0,1:T(8,128)(2,1)} %param.30, f32[8]{0:T(128)S(1)} %copy-done.16), kind=kOutput, calls=%fused_computation.73 | convolution fusion | flops 65680 | bytes 41056 | tf_op jit(solution)/shard_map/dot_general | solution.py:79
  13.4 0.8 %dynamic_slice.17 = f32[256]{0:T(256)S(1)} dynamic-slice(f32[2048]{0:T(1024)} %param.25, s32[]{:T(128)S(6)} %select_n.40), dynamic_slice_sizes={256} | dynamic-slice | bytes 2052 | tf_op jit(solution)/shard_map/dynamic_slice | solution.py:60
  15.1 0.7 copy.61
  15.8 5.6 %all-to-all-start.1 = ((f32[8,2,1152]{2,1,0:T(2,128)}), f32[8,2,1152]{2,1,0:T(2,128)S(1)}, u32[]{:S(2)}, u32[]{:S(2)}) async-start(f32[8,2,1152]{2,1,0:T(2,128)} %copy.61), calls=%async_computation.1 | async-start | bytes 147456 | tf_op jit(solution)/shard_map/all_to_all | solution.py:11
  21.4 6.9 %all-to-all-done.1 = f32[8,2,1152]{2,1,0:T(2,128)S(1)} async-done(((f32[8,2,1152]{2,1,0:T(2,128)}), f32[8,2,1152]{2,1,0:T(2,128)S(1)}, u32[]{:S(2)}, u32[]{:S(2)}) %all-to-all-start.1) | async-done | bytes 73760 | tf_op jit(solution)/shard_map/all_to_all | solution.py:11
  28.5 0.7 copy-done.12
  29.2 0.7 multiply_reduce_fusion.2
  30.1 1.0 %multiply_add_fusion = (f32[2,2,128,256]{3,2,1,0:T(8,128)}, f32[2,2,256]{2,1,0:T(2,128)S(1)}) fusion(f32[2,2,128,256]{3,2,1,0:T(8,128)S(1)} %copy-done.1, f32[2,2,256]{2,1,0:T(2,128)S(1)} %mul.283, f32[2,2,128]{2,1,0:T(2,128)S(1)} %get-tuple-element.7, f32[2,2]{1,0:T(2,128)S(1)} %get-tuple-element.8, f32[2,2,128]{2,1,0:T(2,128)S(1)} %mul.239), kind=kLoop, calls=%fused_computation.17 | loop fusion | flops 654336 | bytes 1060880 | tf_op jit(solution)/shard_map/add | solution.py:91
  31.8 3.3 %all-to-all-start.2 = ((bf16[8,2,512]{2,1,0:T(2,128)(2,1)}), bf16[8,2,512]{2,1,0:T(2,128)(2,1)S(1)}, u32[]{:S(2)}, u32[]{:S(2)}) async-start(bf16[8,2,512]{2,1,0:T(2,128)(2,1)} %broadcast_in_dim.41), calls=%async_computation.2 | async-start | bytes 32768 | tf_op jit(solution)/shard_map/all_to_all | solution.py:11
  35.2 6.5 %all-to-all-done.2 = bf16[8,2,512]{2,1,0:T(2,128)(2,1)S(1)} async-done(((bf16[8,2,512]{2,1,0:T(2,128)(2,1)}), bf16[8,2,512]{2,1,0:T(2,128)(2,1)S(1)}, u32[]{:S(2)}, u32[]{:S(2)}) %all-to-all-start.2) | async-done | bytes 16416 | tf_op jit(solution)/shard_map/all_to_all | solution.py:11
  41.8 0.7 %broadcast_in_dim.42 = bf16[32,16,256]{2,1,0:T(8,128)(2,1)} broadcast(bf16[16,256]{1,0:T(8,128)(2,1)S(1)} %fusion), dimensions={1,2} | broadcast | bytes 270336 | tf_op jit(solution)/shard_map/broadcast_in_dim | solution.py:103
  42.5 2.6 %all-to-all-start.3 = ((bf16[32,16,256]{2,1,0:T(8,128)(2,1)}), bf16[32,16,256]{2,1,0:T(8,128)(2,1)S(1)}, u32[]{:S(2)}, u32[]{:S(2)}) async-start(bf16[32,16,256]{2,1,0:T(8,128)(2,1)} %broadcast_in_dim.42), calls=%async_computation.3 | async-start | bytes 524288 | tf_op jit(solution)/shard_map/all_to_all | solution.py:11
  45.1 0.7 copy-done.11
  46.0 9.7 %all-to-all-done.3 = bf16[32,16,256]{2,1,0:T(8,128)(2,1)S(1)} async-done(((bf16[32,16,256]{2,1,0:T(8,128)(2,1)}), bf16[32,16,256]{2,1,0:T(8,128)(2,1)S(1)}, u32[]{:S(2)}, u32[]{:S(2)}) %all-to-all-start.3) | async-done | bytes 262176 | tf_op jit(solution)/shard_map/all_to_all | solution.py:11
  58.4 0.7 copy.67
  59.1 2.6 %all-to-all-start.4 = ((bf16[32,2,512]{2,1,0:T(2,128)(2,1)}), bf16[32,2,512]{2,1,0:T(2,128)(2,1)S(1)}, u32[]{:S(2)}, u32[]{:S(2)}) async-start(bf16[32,2,512]{2,1,0:T(2,128)(2,1)} %bitcast.15), calls=%async_computation.4 | async-start | bytes 131072 | tf_op jit(solution)/shard_map/all_to_all | solution.py:11
  61.7 7.4 %all-to-all-done.4 = bf16[32,2,512]{2,1,0:T(2,128)(2,1)S(1)} async-done(((bf16[32,2,512]{2,1,0:T(2,128)(2,1)}), bf16[32,2,512]{2,1,0:T(2,128)(2,1)S(1)}, u32[]{:S(2)}, u32[]{:S(2)}) %all-to-all-start.4) | async-done | bytes 65568 | tf_op jit(solution)/shard_map/all_to_all | solution.py:11
  69.2 0.7 add_convert_fusion
  (89 shorter events, 5.5 us)
Async XLA Ops:
  0.6 56.7 %copy-start = (bf16[1,128,2048]{2,1,0:T(8,128)(2,1)S(1)}, bf16[1,128,2048]{2,1,0:T(8,128)(2,1)}, u32[]{:S(2)}) copy-start(bf16[1,128,2048]{2,1,0:T(8,128)(2,1)} %param.39) | copy-start | bytes 1572868
  0.6 14.0 %copy-start.7 = (bf16[256,256]{1,0:T(8,128)(2,1)S(1)}, bf16[256,256]{1,0:T(8,128)(2,1)}, u32[]{:S(2)}) copy-start(bf16[256,256]{1,0:T(8,128)(2,1)} %param.27) | copy-start | bytes 393220
  0.7 11.6 %copy-start.16 = (f32[8]{0:T(128)S(1)}, f32[8]{0:T(128)}, u32[]{:S(2)}) copy-start(f32[8]{0:T(128)} %param.31) | copy-start | bytes 100
  0.7 12.5 %copy-start.14 = (f32[2,2]{1,0:T(2,128)S(1)}, f32[2,2]{1,0:T(2,128)}, u32[]{:S(2)}) copy-start(f32[2,2]{1,0:T(2,128)} %param.24) | copy-start | bytes 52
  0.7 12.6 %copy-start.13 = (s32[2,2]{1,0:T(2,128)S(1)}, s32[2,2]{1,0:T(2,128)}, u32[]{:S(2)}) copy-start(s32[2,2]{1,0:T(2,128)} %param.35) | copy-start | bytes 52
  0.7 14.0 %all-to-all-start = ((bf16[8,2,256]{2,1,0:T(2,128)(2,1)}), bf16[8,2,256]{2,1,0:T(2,128)(2,1)S(1)}, u32[]{:S(2)}, u32[]{:S(2)}) async-start(bf16[8,2,256]{2,1,0:T(2,128)(2,1)} %bitcast.75), calls=%async_computation | async-start | bytes 16384 | tf_op jit(solution)/shard_map/all_to_all | solution.py:11
  8.1 6.7 %copy-start.8 = (bf16[256,256]{1,0:T(8,128)(2,1)S(1)}, bf16[256,256]{1,0:T(8,128)(2,1)}, u32[]{:S(2)}) copy-start(bf16[256,256]{1,0:T(8,128)(2,1)} %param.26) | copy-start | bytes 393220
  8.1 6.8 %copy-start.4 = (bf16[256,512]{1,0:T(8,128)(2,1)S(1)}, bf16[256,512]{1,0:T(8,128)(2,1)}, u32[]{:S(2)}) copy-start(bf16[256,512]{1,0:T(8,128)(2,1)} %param.28) | copy-start | bytes 786436
  13.3 16.5 %copy-start.10 = (f32[2,2]{1,0:T(2,128)}, f32[2,2]{1,0:T(2,128)S(1)}, u32[]{:S(2)}) copy-start(f32[2,2]{1,0:T(2,128)S(1)} %get-tuple-element.9) | copy-start | bytes 52
  14.8 15.2 %copy-start.1 = (f32[2,2,128,256]{3,2,1,0:T(8,128)S(1)}, f32[2,2,128,256]{3,2,1,0:T(8,128)}, u32[]{:S(2)}) copy-start(f32[2,2,128,256]{3,2,1,0:T(8,128)} %param.22) | copy-start | bytes 1572868
  15.8 12.5 %all-to-all-start.1 = ((f32[8,2,1152]{2,1,0:T(2,128)}), f32[8,2,1152]{2,1,0:T(2,128)S(1)}, u32[]{:S(2)}, u32[]{:S(2)}) async-start(f32[8,2,1152]{2,1,0:T(2,128)} %copy.61), calls=%async_computation.1 | async-start | bytes 147456 | tf_op jit(solution)/shard_map/all_to_all | solution.py:11
  28.5 0.7 copy-start.12
  30.0 11.6 %copy-start.5 = (bf16[512,256]{1,0:T(8,128)(2,1)S(1)}, bf16[512,256]{1,0:T(8,128)(2,1)}, u32[]{:S(2)}) copy-start(bf16[512,256]{1,0:T(8,128)(2,1)} %param.32) | copy-start | bytes 786436
  31.8 9.9 %all-to-all-start.2 = ((bf16[8,2,512]{2,1,0:T(2,128)(2,1)}), bf16[8,2,512]{2,1,0:T(2,128)(2,1)S(1)}, u32[]{:S(2)}, u32[]{:S(2)}) async-start(bf16[8,2,512]{2,1,0:T(2,128)(2,1)} %broadcast_in_dim.41), calls=%async_computation.2 | async-start | bytes 32768 | tf_op jit(solution)/shard_map/all_to_all | solution.py:11
  42.5 13.2 %all-to-all-start.3 = ((bf16[32,16,256]{2,1,0:T(8,128)(2,1)}), bf16[32,16,256]{2,1,0:T(8,128)(2,1)S(1)}, u32[]{:S(2)}, u32[]{:S(2)}) async-start(bf16[32,16,256]{2,1,0:T(8,128)(2,1)} %broadcast_in_dim.42), calls=%async_computation.3 | async-start | bytes 524288 | tf_op jit(solution)/shard_map/all_to_all | solution.py:11
  45.1 0.7 copy-start.11
  45.1 0.7 %copy-start.9 = (f32[2048]{0:T(1024)S(1)}, f32[2048]{0:T(1024)}, u32[]{:S(2)}) copy-start(f32[2048]{0:T(1024)} %param.33) | copy-start | bytes 24580
  55.9 0.7 %copy-start.15 = (bf16[2048,4]{0,1:T(4,128)(2,1)S(1)}, bf16[2048,4]{0,1:T(4,128)(2,1)}, u32[]{:S(2)}) copy-start(bf16[2048,4]{0,1:T(4,128)(2,1)} %param.34) | copy-start | bytes 49156
  55.9 1.0 %copy-start.6 = (bf16[256,512]{1,0:T(8,128)(2,1)S(1)}, bf16[256,512]{1,0:T(8,128)(2,1)}, u32[]{:S(2)}) copy-start(bf16[256,512]{1,0:T(8,128)(2,1)} %param.40) | copy-start | bytes 786436
  56.0 1.1 %copy-start.2 = (bf16[1,2048,128]{2,1,0:T(8,128)(2,1)S(1)}, bf16[1,2048,128]{2,1,0:T(8,128)(2,1)}, u32[]{:S(2)}) copy-start(bf16[1,2048,128]{2,1,0:T(8,128)(2,1)} %param.37) | copy-start | bytes 1572868
  56.8 1.0 %copy-start.3 = (bf16[1,2048,128]{2,1,0:T(8,128)(2,1)S(1)}, bf16[1,2048,128]{2,1,0:T(8,128)(2,1)}, u32[]{:S(2)}) copy-start(bf16[1,2048,128]{2,1,0:T(8,128)(2,1)} %param.38) | copy-start | bytes 1572868
  59.1 10.0 %all-to-all-start.4 = ((bf16[32,2,512]{2,1,0:T(2,128)(2,1)}), bf16[32,2,512]{2,1,0:T(2,128)(2,1)S(1)}, u32[]{:S(2)}, u32[]{:S(2)}) async-start(bf16[32,2,512]{2,1,0:T(2,128)(2,1)} %bitcast.15), calls=%async_computation.4 | async-start | bytes 131072 | tf_op jit(solution)/shard_map/all_to_all | solution.py:11

commit v2 on v1

--- a/solution.py
+++ b/solution.py
@@ -1,14 +1,237 @@
+import functools
+
 import jax
 import jax.numpy as jnp
 from jax import lax
+from jax.experimental import pallas as pl
+from jax.experimental.pallas import tpu as pltpu
 from jax.sharding import PartitionSpec as P
 
 eps = 1e-06
 BOTH = ("ep", "tp")
+f32, bf16 = jnp.float32, jnp.bfloat16
+VMEM_BYTES = 12 << 20
 
 
 def exchange(chunks, axes):
     return lax.all_to_all(chunks, axes, split_axis=0, concat_axis=0, tiled=True)
+
+
+def shaped(*dims, dtype=f32):
+    return jax.ShapeDtypeStruct(dims, dtype)
+
+
+def run(body, outs, name, scalars, *arrays):
+    specs = [pl.BlockSpec(memory_space=pltpu.SMEM)] * len(scalars)
+    specs += [pl.BlockSpec(memory_space=pltpu.VMEM)] * len(arrays)
+    return pl.pallas_call(
+        body,
+        out_shape=outs,
+        in_specs=specs,
+        name=name,
+        compiler_params=pltpu.CompilerParams(vmem_limit_bytes=VMEM_BYTES),
+    )(*scalars, *arrays)
+
+
+def dot(left, right, dims=((1,), (0,))):
+    return lax.dot_general(left, right, (dims, ((), ())), preferred_element_type=f32)
+
+
+def project_body(spread, gain, w_query, w_key, w_value, picks, out):
+    scaled = (spread[...].astype(f32) * gain[...]).astype(bf16)
+    at, own = 0, out.shape[1]
+    for w in (w_query, w_key, w_value):
+        sums = dot(scaled, w[...])
+        for b in range(out.shape[0]):
+            out[b, :, at : at + w.shape[1]] = sums[b * own : (b + 1) * own]
+        at += w.shape[1]
+    for b in range(out.shape[0]):
+        out[b, :, at:] = picks[b]
+
+
+def memory_body(parts, inverse, decay, inflow, state_c, kept_n, heads_out, new_n_out, qkv_out, coef_out):
+    blocks, own, _ = parts.shape
+    head_count, dqk, dv = state_c.shape[1:]
+    packed = head_count * (2 * dqk + dv)
+    total = parts[0, :, :packed]
+    for b in range(1, blocks):
+        total += parts[b, :, :packed]
+    for b in range(blocks):
+        coef_out[b * own : (b + 1) * own, :] = parts[b, :, packed:]
+    qkv = (total * inverse[...]).astype(bf16).astype(f32)
+    qkv_out[...] = qkv
+    for i in range(own):
+        for h in range(head_count):
+            q = qkv[i : i + 1, h * dqk : (h + 1) * dqk]
+            at = (head_count + h) * dqk
+            k = qkv[i : i + 1, at : at + dqk] * dqk ** (-0.5)
+            at = 2 * head_count * dqk + h * dv
+            v = qkv[i : i + 1, at : at + dv]
+            kept, flow = decay[i : i + 1, h : h + 1], inflow[i : i + 1, h : h + 1]
+            new_n = kept_n[i, h : h + 1, :] + flow * k
+            new_n_out[i, h : h + 1, :] = new_n
+            recalled = lax.dot_general(
+                q, state_c[i, h], (((1,), (0,)), ((), ())),
+                preferred_element_type=f32, precision=lax.Precision.HIGHEST,
+            )
+            numer = kept * recalled + (flow * jnp.sum(q * k, axis=1, keepdims=True)) * v
+            denom = jnp.maximum(jnp.abs(jnp.sum(q * new_n, axis=1, keepdims=True)), 1.0)
+            head = (numer / denom).astype(bf16)
+            for d in range(heads_out.shape[0]):
+                heads_out[d, i : i + 1, h * dv : (h + 1) * dv] = head
+
+
+def output_body(tp_ref, heads, near, far, spread, out):
+    own = heads.shape[1]
+    tp_count = heads.shape[0] * own // spread.shape[0]
+    half, some = out.shape[2], out.shape[1]
+    rank = tp_ref[0]
+    side, part = rank % 2, rank // 2
+    blocks = some // own
+    at = pl.ds(pl.multiple_of(side * half, 128), half)
+    tokens = spread[:, at].astype(f32)
+    total = jnp.where(part == 0, tokens[:some], tokens[some:])
+    for d in range(tp_count):
+        source = rank ^ d
+        pieces = [heads[(part * blocks + b) * tp_count + source].astype(f32) for b in range(blocks)]
+        left = jnp.concatenate(pieces, axis=0).astype(bf16)
+        total += dot(left, (far if d // 2 else near)[d % 2])
+    total = total.astype(bf16)
+    for d in range(out.shape[0]):
+        out[d] = total
+
+
+def experts_body(
+    ranks, every, coef, gain, w_group, w_dense_gate, w_gate, w_up, w_down, w_dense,
+    out, own_out, normed_buf, total_buf, *, per_group, ep_count,
+):
+    seqs, width = normed_buf.shape
+    count, some, half = every.shape
+    tp_count = count // ep_count
+    own, share = out.shape[1], out.shape[2]
+    ep_rank, tp_rank = ranks[0], ranks[1]
+    halves = []
+    for part in range(2):
+        tiles = [every[e * tp_count + part * 2 + s].astype(f32) for e in range(ep_count) for s in range(2)]
+        halves.append(jnp.concatenate(tiles, axis=1))
+    residual = jnp.concatenate(halves, axis=0)
+    inverse = lax.rsqrt(jnp.mean(residual * residual, axis=-1, keepdims=True) + eps)
+    normed = (residual * inverse * gain[...]).astype(bf16)
+    normed_buf[...] = normed.astype(f32)
+    total_buf[...] = residual
+    columns = pl.ds(pl.multiple_of(tp_rank * share, 128), share)
+    mine = total_buf[:, columns]
+    row = lax.broadcasted_iota(jnp.int32, mine.shape, 0)
+    for i in range(own):
+        held = jnp.where(row == ep_rank * own + i, mine, 0.0)
+        own_out[i : i + 1, :] = jnp.sum(held, axis=0, keepdims=True)
+    logits = dot(normed, w_group[...], ((1,), (1,)))
+    powers = jnp.exp(logits - jnp.max(logits, axis=1, keepdims=True))
+    lane = lax.broadcasted_iota(jnp.int32, logits.shape, 1)
+    chosen = jnp.sum(jnp.where(lane == ep_rank // per_group, powers, 0.0), axis=1, keepdims=True)
+    route = chosen / jnp.sum(powers, axis=1, keepdims=True) * coef[:, 0:1]
+    gate_act = dot(normed, w_gate[0])
+    up_act = dot(normed, w_up[0])
+    hidden = (gate_act * jax.nn.sigmoid(gate_act) * up_act).astype(bf16)
+    total_buf[...] = route * dot(hidden, w_down[0])
+    rows = w_dense.shape[0]
+    some_in = normed_buf[:, pl.ds(pl.multiple_of(ep_rank * rows, 128), rows)].astype(bf16)
+    gate = jnp.sum(normed.astype(f32) * w_dense_gate[...].astype(f32), axis=1, keepdims=True)
+    total_buf[:, columns] += jax.nn.sigmoid(gate) * dot(some_in, w_dense[...])
+    for b in range(ep_count):
+        for t in range(tp_count):
+            piece = total_buf[b * own : (b + 1) * own, t * share : (t + 1) * share]
+            out[b * tp_count + t] = piece.astype(bf16)
+
+
+def fast_device(
+    tokens, state_c, state_n, state_m, mix_gain, w_query, w_key, w_value, w_input_gate, w_forget_gate,
+    forget_bias, w_output, moe_gain, w_group, expert_ids, expert_weight, w_exp_gate, w_exp_up,
+    w_exp_down, w_dense, w_dense_gate,
+):
+    own, width = tokens.shape
+    tp_count, ep_count = lax.axis_size("tp"), lax.axis_size("ep")
+    tp_rank, ep_rank = lax.axis_index("tp"), lax.axis_index("ep")
+    every_count = ep_count * tp_count
+    seqs, (rows, qk_cols), v_cols = own * ep_count, w_query.shape, w_value.shape[1]
+    head_count, share, half = state_m.shape[1], width // tp_count, w_output.shape[1] // 2
+    tp_ref, ranks = tp_rank.reshape(1), jnp.stack([ep_rank, tp_rank])
+    gain = mix_gain.reshape(1, width)
+    packed = 2 * qk_cols + v_cols
+    with jax.named_scope("r1"):
+        spread = exchange(tokens.reshape(own, ep_count, rows).transpose(1, 0, 2), "ep")
+    spread = spread.reshape(seqs, rows)
+    side = tp_rank % 2
+    with jax.named_scope("swap"):
+        given = lax.dynamic_slice_in_dim(w_output, (1 - side) * half, half, 1)
+        taken = lax.ppermute(given, "tp", [(d, d ^ 1) for d in range(tp_count)])
+    with jax.named_scope("cross"):
+        pair = jnp.stack([lax.dynamic_slice_in_dim(w_output, side * half, half, 1), taken])
+        far = lax.ppermute(pair, "tp", [(d, d ^ 2) for d in range(tp_count)])
+    gain_rows = lax.dynamic_slice_in_dim(gain, ep_rank * rows, rows, 1)
+    expert_of = jnp.arange(ep_count, dtype=jnp.int32)
+    shares = expert_weight / jnp.sum(expert_weight, axis=1, keepdims=True)
+    picks = jnp.where(expert_ids[None, :, :] == expert_of[:, None, None], shares[None], 0.0)
+    picks = jnp.broadcast_to(jnp.sum(picks, axis=2)[..., None], (ep_count, own, 128))
+    wide = tokens.astype(f32)
+    inverse = lax.rsqrt(jnp.mean(wide * wide, axis=-1, keepdims=True) + eps)
+    normed = (wide * inverse * mix_gain).astype(bf16)
+    gate_all = jnp.dot(normed, w_input_gate, preferred_element_type=f32)
+    forget_all = jax.nn.log_sigmoid(
+        jnp.dot(normed, w_forget_gate, preferred_element_type=f32) + forget_bias
+    )
+    in_gate = lax.dynamic_slice_in_dim(gate_all, tp_rank * head_count, head_count, 1)
+    forget = lax.dynamic_slice_in_dim(forget_all, tp_rank * head_count, head_count, 1)
+    new_m = jnp.maximum(forget + state_m, in_gate)
+    decay = jnp.exp(forget + state_m - new_m)
+    inflow = jnp.exp(in_gate - new_m)
+    kept_n = decay[..., None] * state_n
+    sums = run(
+        project_body, shaped(ep_count, own, packed + 128), "project", (),
+        spread, gain_rows, w_query, w_key, w_value, picks,
+    )
+    with jax.named_scope("r2"):
+        parts = exchange(sums, "ep")
+    heads, new_n, qkv, coef = run(
+        memory_body,
+        (
+            shaped(every_count, own, v_cols, dtype=bf16), shaped(*state_n.shape),
+            shaped(own, packed), shaped(seqs, 128),
+        ),
+        "memory", (), parts, inverse, decay, inflow, state_c, kept_n,
+    )
+    with jax.named_scope("r3"):
+        heads = exchange(heads, BOTH)
+    k_heads = qkv[:, qk_cols : 2 * qk_cols].reshape(own, head_count, -1)
+    k_heads = k_heads * k_heads.shape[-1] ** (-0.5)
+    v_heads = qkv[:, 2 * qk_cols :].reshape(own, head_count, -1)
+    new_c = (
+        decay[..., None, None] * state_c
+        + (inflow[..., None] * k_heads)[..., :, None] * v_heads[..., None, :]
+    )
+    out = run(
+        output_body, shaped(every_count, seqs // 2, half, dtype=bf16), "output", (tp_ref,),
+        heads, pair, far, spread,
+    )
+    with jax.named_scope("r4"):
+        every = exchange(out, BOTH)
+    last, own_rows = pl.pallas_call(
+        functools.partial(
+            experts_body, per_group=ep_count // w_group.shape[1], ep_count=ep_count
+        ),
+        out_shape=(shaped(every_count, own, share, dtype=bf16), shaped(own, share)),
+        in_specs=[pl.BlockSpec(memory_space=pltpu.SMEM)] + [pl.BlockSpec(memory_space=pltpu.VMEM)] * 9,
+        scratch_shapes=[pltpu.VMEM((seqs, width), f32)] * 2,
+        name="experts",
+        compiler_params=pltpu.CompilerParams(vmem_limit_bytes=VMEM_BYTES),
+    )(
+        ranks, every, coef, moe_gain.reshape(1, width), w_group.T, w_dense_gate.reshape(1, width),
+        w_exp_gate, w_exp_up, w_exp_down, w_dense,
+    )
+    with jax.named_scope("r5"):
+        last = exchange(last, BOTH)
+    mixed = (own_rows + jnp.sum(last.astype(f32), axis=0)).astype(bf16)
+    return (mixed, new_c, new_n, new_m)
 
 
 def rms_norm(values, gain):
@@ -17,7 +240,7 @@
     return (widened * inverse * gain).astype(jnp.bfloat16)
 
 
-def per_device(
+def plain_device(
     tokens,
     state_c,
     state_n,
@@ -40,7 +263,6 @@
     w_dense,
     w_dense_gate,
 ):
-    f32, bf16 = jnp.float32, jnp.bfloat16
     own, width = tokens.shape
     tp_count = lax.axis_size("tp")
     ep_count = lax.axis_size("ep")
@@ -131,6 +353,19 @@
     return (mixed, new_c, new_n, new_m)
 
 
+def per_device(*args):
+    rows, cols, experts_here = args[5].shape[0], args[11].shape[1], args[16].shape[0]
+    seqs = args[0].shape[0] * lax.axis_size("ep")
+    fits = (
+        lax.axis_size("tp") == 4
+        and seqs % 16 == 0
+        and rows % 128 == 0
+        and cols % 256 == 0
+        and experts_here == 1
+    )
+    return (fast_device if fits else plain_device)(*args)
+
+
 def solution(mesh):
     placed = (
         P("ep", None),

time: 70.7 us -> 61 us (0.86)
  Pallas kernels: 0 us -> 4.51 us
  other arithmetic: 6.71 us -> 2.49 us
  local copies, waits for them, and re-layouts: 6.55 us -> 3.27 us
  matrix products: 3.27 us -> 0.27 us
  waiting for transfers between devices: 30.8 us -> 28.7 us
  starting transfers between devices: 21.5 us -> 20.5 us
    pallas_call x0 -> x4, Pallas kernels: none -> 4.51 us  [the longest x3 2.69 us: run(): pl.pallas_call(body, out_shape=outs, in_specs=specs, name=name, compiler_...]
    dot_general x11 -> x2, matrix products: 3.27 us -> 0.27 us  [the longest x1 0.14 us: fast_device(): jnp.dot(normed, w_forget_gate, preferred_element_type=f32) + forget_bias]
    all_to_all x5, starting transfers between devices: 21.5 us -> 18.8 us  [exchange(): return lax.all_to_all(chunks, axes, split_axis=0, concat_axis=0, tiled=True)]
    reduce_sum x10 -> x4, other arithmetic: 2.79 us -> 0.41 us  [the longest x1 0.13 us: fast_device(): inverse = lax.rsqrt(jnp.mean(wide * wide, axis=-1, keepdims=True) + eps)]
    all_to_all x5, waiting for transfers between devices: 30.8 us -> 28.7 us  [exchange(): return lax.all_to_all(chunks, axes, split_axis=0, concat_axis=0, tiled=True)]
    ppermute x0 -> x2, starting transfers between devices: none -> 1.63 us  [the longest x1 1.56 us: fast_device(): far = lax.ppermute(pair, 'tp', [(d, d ^ 2) for d in range(tp_count)])]
    broadcast_in_dim x4 -> x1, local copies, waits for them, and re-layouts: 1.41 us -> 0.07 us  [fast_device(): jnp.broadcast_to(jnp.sum(picks, axis=2)[..., None], (ep_count, own, 128))]
    another operation x1 -> x2, local copies, waits for them, and re-layouts: 0.09 us -> 1.12 us  [the longest x1 1.04 us: fast_device(): jnp.stack([lax.dynamic_slice_in_dim(w_output, side * half, half, 1), taken])]
  transfers between devices with their start and end apart: 5 -> 7, of which waited for: 5 -> 5; matrix products, arithmetic and copies ran while one was open for 9% -> 6% of each run, Pallas kernels for 0% -> 3%
where the time goes in v2:
time: 61 us; the launch traced here: 60.5 us
  waiting for transfers between devices  28.7 us (47%)
  starting transfers between devices  20.5 us (34%)
  Pallas kernels  4.51 us (7%)
  local copies, waits for them, and re-layouts  3.27 us (5%)
  other arithmetic  2.49 us (4%)
  between operations  0.88 us (1%)
    all_to_all x5, waiting for transfers between devices, exchange(): return lax.all_to_all(chunks, axes, split_axis=0, concat_axis=0, tiled=True)  28.7 us
    all_to_all x5, starting transfers between devices, exchange(): return lax.all_to_all(chunks, axes, split_axis=0, concat_axis=0, tiled=True)  18.8 us
    pallas_call x3, Pallas kernels, run(): pl.pallas_call(body, out_shape=outs, in_specs=specs, name=name, compiler_...  2.69 us
    unnamed x42, local copies, waits for them, and re-layouts  1.86 us
    pallas_call x1, Pallas kernels, fast_device(): pl.pallas_call(functools.partial(experts_body, per_group=ep_count // w_gr...  1.82 us
    ppermute x1, starting transfers between devices, fast_device(): far = lax.ppermute(pair, 'tp', [(d, d ^ 2) for d in range(tp_count)])  1.56 us
  transfers between devices with their start and end apart: 7, of which 5 were waited for; matrix products, arithmetic and copies ran while one was open for 6% of the time, Pallas kernels for 3%

profile of v2, /device:TPU:0, one launch (start us, length us, event | category | flops | bytes accessed | tf_op | source)
XLA Modules:
  0.0 60.5 jit_solution(1332471798138786211)
XLA Ops:
  0.6 7.3 %all-to-all-start = ((bf16[8,2,256]{2,1,0:T(2,128)(2,1)}), bf16[8,2,256]{2,1,0:T(2,128)(2,1)S(1)}, u32[]{:S(2)}, u32[]{:S(2)}) async-start(bf16[8,2,256]{2,1,0:T(2,128)(2,1)} %bitcast.21), calls=%async_computation | async-start | bytes 16384 | tf_op jit(solution)/shard_map/r1/all_to_all | solution.py:17
  8.0 1.0 %dynamic-slice_bitcast_fusion = (bf16[1,512,128]{2,1,0:T(8,128)(2,1)S(1)}, bf16[512,128]{1,0:T(8,128)(2,1)S(1)}) fusion(bf16[512,256]{1,0:T(8,128)(2,1)} %param.32, s32[]{:T(128)S(6)} %select_n.34, s32[]{:T(128)S(6)} %select_n.35), kind=kLoop, calls=%fused_computation.5 | loop fusion | bytes 524296 | tf_op jit(solution)/shard_map/cross/stack | solution.py:169
  9.2 0.1 fusion.1
  9.4 0.1 fusion.9
  9.6 0.1 fusion.5
  9.7 0.5 copy-done.15
  10.4 0.5 copy-done.16
  11.2 0.6 copy-done.18
  12.1 2.3 %all-to-all-done = bf16[8,2,256]{2,1,0:T(2,128)(2,1)S(1)} async-done(((bf16[8,2,256]{2,1,0:T(2,128)(2,1)}), bf16[8,2,256]{2,1,0:T(2,128)(2,1)S(1)}, u32[]{:S(2)}, u32[]{:S(2)}) %all-to-all-start) | async-done | bytes 8224 | tf_op jit(solution)/shard_map/r1/all_to_all | solution.py:17
  14.6 0.8 %project.1 = f32[8,2,1152]{2,1,0:T(2,128)} custom-call(bf16[16,256]{1,0:T(8,128)(2,1)S(1)} %reshape.63.spread, f32[1,256]{1,0:T(1,128)S(1)} %bitcast.19, bf16[256,256]{1,0:T(8,128)(2,1)S(1)} %copy-done.7, bf16[256,256]{1,0:T(8,128)(2,1)S(1)} %copy-done.8, bf16[256,512]{1,0:T(8,128)(2,1)S(1)} %copy-done.6, f32[8,2,128]{2,1,0:T(2,128)S(1)} %broadcast_in_dim.16.picks), custom_call_target="tpu_custom_call" | custom-call | tf_op jit(solution)/shard_map/project/pallas_call | solution.py:27
  15.4 3.7 %all-to-all-start.1 = ((f32[8,2,1152]{2,1,0:T(2,128)}), f32[8,2,1152]{2,1,0:T(2,128)S(1)}, u32[]{:S(2)}, u32[]{:S(2)}) async-start(f32[8,2,1152]{2,1,0:T(2,128)} %project.1), calls=%async_computation.1 | async-start | bytes 147456 | tf_op jit(solution)/shard_map/r2/all_to_all | solution.py:17
  19.2 1.6 %collective-permute-start.1 = (bf16[2,512,128]{2,1,0:T(8,128)(2,1)S(1)}, bf16[2,512,128]{2,1,0:T(8,128)(2,1)S(1)}, u32[]{:S(2)}, u32[]{:S(2)}) collective-permute-start(bf16[2,512,128]{2,1,0:T(8,128)(2,1)S(1)} %pad_maximum_fusion.near), channel_id=1, source_target_pairs={{0,2},{1,3},{2,0},{3,1},{4,6},{5,7},{6,4},{7,5},{8,10},{9,11},{10,... | collective-permute-start | bytes 786440 | tf_op jit(solution)/shard_map/cross/ppermute | solution.py:170
  20.8 5.2 %all-to-all-done.1.parts = f32[8,2,1152]{2,1,0:T(2,128)S(1)} async-done(((f32[8,2,1152]{2,1,0:T(2,128)}), f32[8,2,1152]{2,1,0:T(2,128)S(1)}, u32[]{:S(2)}, u32[]{:S(2)}) %all-to-all-start.1) | async-done | bytes 73760 | tf_op jit(solution)/shard_map/r2/all_to_all | solution.py:17
  26.1 1.0 %memory.1 = (bf16[32,2,512]{2,1,0:T(2,128)(2,1)}, f32[2,2,128]{2,1,0:T(2,128)}, f32[2,1024]{1,0:T(2,128)S(1)}, f32[16,128]{1,0:T(8,128)S(1)}) custom-call(f32[8,2,1152]{2,1,0:T(2,128)S(1)} %all-to-all-done.1.parts, f32[2,1]{1,0:T(2,128)S(1)} %copy.29.inverse, f32[2,2]{1,0:T(2,128)S(1)} %subtract_exponential_fusion.1.decay, ...), custom_call_target="tpu_custom_call" | custom-call | tf_op jit(solution)/shard_map/memory/pallas_call | solution.py:27
  27.1 2.7 %all-to-all-start.2 = ((bf16[32,2,512]{2,1,0:T(2,128)(2,1)}), bf16[32,2,512]{2,1,0:T(2,128)(2,1)S(1)}, u32[]{:S(2)}, u32[]{:S(2)}) async-start(bf16[32,2,512]{2,1,0:T(2,128)(2,1)} %get-tuple-element.10), calls=%async_computation.2 | async-start | bytes 131072 | tf_op jit(solution)/shard_map/r3/all_to_all | solution.py:17
  30.0 7.3 %all-to-all-done.2.heads = bf16[32,2,512]{2,1,0:T(2,128)(2,1)S(1)} async-done(((bf16[32,2,512]{2,1,0:T(2,128)(2,1)}), bf16[32,2,512]{2,1,0:T(2,128)(2,1)S(1)}, u32[]{:S(2)}, u32[]{:S(2)}) %all-to-all-start.2) | async-done | bytes 65568 | tf_op jit(solution)/shard_map/r3/all_to_all | solution.py:17
  37.2 0.8 %output.1 = bf16[32,8,128]{2,1,0:T(8,128)(2,1)} custom-call(s32[1]{0:T(128)} %bitcast.1.tp_ref, bf16[32,2,512]{2,1,0:T(2,128)(2,1)S(1)} %all-to-all-done.2.heads, bf16[2,512,128]{2,1,0:T(8,128)(2,1)S(1)} %pad_maximum_fusion.near, bf16[2,512,128]{2,1,0:T(8,128)(2,1)S(1)} %collective-permute-done.1.far, bf16[16,256]{1,0:T(8,128)(2,1)S(1)} %reshape.63.spread), custom_call_target="tpu_custom_call" | custom-call | tf_op jit(solution)/shard_map/output/pallas_call | solution.py:27
  38.1 2.6 %all-to-all-start.3 = ((bf16[32,8,128]{2,1,0:T(8,128)(2,1)}), bf16[32,8,128]{2,1,0:T(8,128)(2,1)S(1)}, u32[]{:S(2)}, u32[]{:S(2)}) async-start(bf16[32,8,128]{2,1,0:T(8,128)(2,1)} %output.1), calls=%async_computation.3 | async-start | bytes 131072 | tf_op jit(solution)/shard_map/r4/all_to_all | solution.py:17
  40.7 7.3 %all-to-all-done.3.every = bf16[32,8,128]{2,1,0:T(8,128)(2,1)S(1)} async-done(((bf16[32,8,128]{2,1,0:T(8,128)(2,1)}), bf16[32,8,128]{2,1,0:T(8,128)(2,1)S(1)}, u32[]{:S(2)}, u32[]{:S(2)}) %all-to-all-start.3) | async-done | bytes 65568 | tf_op jit(solution)/shard_map/r4/all_to_all | solution.py:17
  48.1 1.8 %experts.1 = (bf16[32,2,512]{2,1,0:T(2,128)(2,1)}, f32[2,512]{1,0:T(2,128)S(1)}) custom-call(s32[2]{0:T(128)S(1)} %pad_add_fusion.ranks, bf16[32,8,128]{2,1,0:T(8,128)(2,1)S(1)} %all-to-all-done.3.every, f32[16,128]{1,0:T(8,128)S(1)} %get-tuple-element.11.coef, f32[1,2048]{1,0:T(1,128)S(1)} %bitcast.18, bf16[4,2048]{1,0:T(4,128)(2,1)S(1)} %bitcast.17, ...), custom_call_target="tpu_custom_call" | custom-call | tf_op jit(solution)/shard_map/experts/pallas_call | solution.py:218
  49.9 2.5 %all-to-all-start.4 = ((bf16[32,2,512]{2,1,0:T(2,128)(2,1)}), bf16[32,2,512]{2,1,0:T(2,128)(2,1)S(1)}, u32[]{:S(2)}, u32[]{:S(2)}) async-start(bf16[32,2,512]{2,1,0:T(2,128)(2,1)} %get-tuple-element.13), calls=%async_computation.4 | async-start | bytes 131072 | tf_op jit(solution)/shard_map/r5/all_to_all | solution.py:17
  52.5 0.9 %multiply_add_fusion = f32[2,2,128,256]{3,2,1,0:T(8,128)} fusion(f32[2,2,128,256]{3,2,1,0:T(8,128)S(1)} %copy-done.1, f32[2,2,256]{2,1,0:T(2,128)S(1)} %mul.99, f32[2,2,128]{2,1,0:T(2,128)S(1)} %broadcast_multiply_fusion, f32[2,2]{1,0:T(2,128)S(1)} %subtract_exponential_fusion.1.decay), kind=kLoop, calls=%fused_computation.2 | loop fusion | flops 393216 | bytes 1054736 | tf_op jit(solution)/shard_map/add | solution.py:209
  53.4 6.5 %all-to-all-done.4 = bf16[32,2,512]{2,1,0:T(2,128)(2,1)S(1)} async-done(((bf16[32,2,512]{2,1,0:T(2,128)(2,1)}), bf16[32,2,512]{2,1,0:T(2,128)(2,1)S(1)}, u32[]{:S(2)}, u32[]{:S(2)}) %all-to-all-start.4) | async-done | bytes 65568 | tf_op jit(solution)/shard_map/r5/all_to_all | solution.py:17
  60.0 0.6 add_convert_fusion
  (64 shorter events, 1.5 us)
Async XLA Ops:
  0.6 8.8 %copy-start = (bf16[2048,8]{0,1:T(8,128)(2,1)S(1)}, bf16[2048,8]{0,1:T(8,128)(2,1)}, u32[]{:S(2)}) copy-start(bf16[2048,8]{0,1:T(8,128)(2,1)} %param.29) | copy-start | bytes 98308
  0.6 13.8 %all-to-all-start = ((bf16[8,2,256]{2,1,0:T(2,128)(2,1)}), bf16[8,2,256]{2,1,0:T(2,128)(2,1)S(1)}, u32[]{:S(2)}, u32[]{:S(2)}) async-start(bf16[8,2,256]{2,1,0:T(2,128)(2,1)} %bitcast.21), calls=%async_computation | async-start | bytes 16384 | tf_op jit(solution)/shard_map/r1/all_to_all | solution.py:17
  8.0 1.2 %copy-start.11 = (bf16[2,2048]{1,0:T(2,128)(2,1)S(1)}, bf16[2,2048]{1,0:T(2,128)(2,1)}, u32[]{:S(2)}) copy-start(bf16[2,2048]{1,0:T(2,128)(2,1)} %param.21) | copy-start | bytes 24580
  8.0 1.3 %copy-start.12 = (f32[2048]{0:T(1024)S(1)}, f32[2048]{0:T(1024)}, u32[]{:S(2)}) copy-start(f32[2048]{0:T(1024)} %param.25) | copy-start | bytes 24580
  8.0 1.6 %copy-start.19 = (bf16[2048,8]{0,1:T(8,128)(2,1)S(1)}, bf16[2048,8]{0,1:T(8,128)(2,1)}, u32[]{:S(2)}) copy-start(bf16[2048,8]{0,1:T(8,128)(2,1)} %param.30) | copy-start | bytes 98308
  8.0 1.6 %copy-start.20 = (f32[8]{0:T(128)S(1)}, f32[8]{0:T(128)}, u32[]{:S(2)}) copy-start(f32[8]{0:T(128)} %param.31) | copy-start | bytes 100
  8.0 6.6 %copy-start.6 = (bf16[256,512]{1,0:T(8,128)(2,1)S(1)}, bf16[256,512]{1,0:T(8,128)(2,1)}, u32[]{:S(2)}) copy-start(bf16[256,512]{1,0:T(8,128)(2,1)} %w_value.1) | copy-start | bytes 786436
  8.0 6.6 %copy-start.8 = (bf16[256,256]{1,0:T(8,128)(2,1)S(1)}, bf16[256,256]{1,0:T(8,128)(2,1)}, u32[]{:S(2)}) copy-start(bf16[256,256]{1,0:T(8,128)(2,1)} %w_key.1) | copy-start | bytes 393220
  9.1 5.5 %copy-start.7 = (bf16[256,256]{1,0:T(8,128)(2,1)S(1)}, bf16[256,256]{1,0:T(8,128)(2,1)}, u32[]{:S(2)}) copy-start(bf16[256,256]{1,0:T(8,128)(2,1)} %w_query.1) | copy-start | bytes 393220
  9.1 10.0 %collective-permute-start = (bf16[512,128]{1,0:T(8,128)(2,1)S(1)}, bf16[512,128]{1,0:T(8,128)(2,1)S(1)}, u32[]{:S(2)}, u32[]{:S(2)}) collective-permute-start(bf16[512,128]{1,0:T(8,128)(2,1)S(1)} %get-tuple-element.20), channel_id=1, source_target_pairs={{0,1},{1,0},{2,3},{3,2},{4,5},{5,4},{6,7},{7,6},{8,9},{9,8},{10,11... | collective-permute-start | bytes 393224 | tf_op jit(solution)/shard_map/swap/ppermute | solution.py:167
  14.6 11.5 %copy-start.1 = (f32[2,2,128,256]{3,2,1,0:T(8,128)S(1)}, f32[2,2,128,256]{3,2,1,0:T(8,128)}, u32[]{:S(2)}) copy-start(f32[2,2,128,256]{3,2,1,0:T(8,128)} %state_c.1) | copy-start | bytes 1572868
  15.4 10.6 %all-to-all-start.1 = ((f32[8,2,1152]{2,1,0:T(2,128)}), f32[8,2,1152]{2,1,0:T(2,128)S(1)}, u32[]{:S(2)}, u32[]{:S(2)}) async-start(f32[8,2,1152]{2,1,0:T(2,128)} %project.1), calls=%async_computation.1 | async-start | bytes 147456 | tf_op jit(solution)/shard_map/r2/all_to_all | solution.py:17
  19.1 1.6 %copy-start.17 = (f32[2,2,128]{2,1,0:T(2,128)S(1)}, f32[2,2,128]{2,1,0:T(2,128)}, u32[]{:S(2)}) copy-start(f32[2,2,128]{2,1,0:T(2,128)} %param.23) | copy-start | bytes 6148
  19.1 10.7 %copy-start.13 = (bf16[2048]{0:T(1024)(128)(2,1)S(1)}, bf16[2048]{0:T(1024)(128)(2,1)}, u32[]{:S(2)}) copy-start(bf16[2048]{0:T(1024)(128)(2,1)} %param.41) | copy-start | bytes 12292
  19.1 28.9 %copy-start.5 = (bf16[256,512]{1,0:T(8,128)(2,1)S(1)}, bf16[256,512]{1,0:T(8,128)(2,1)}, u32[]{:S(2)}) copy-start(bf16[256,512]{1,0:T(8,128)(2,1)} %w_dense.1) | copy-start | bytes 786436
  19.1 28.9 %copy-start.9 = (bf16[2048,4]{0,1:T(4,128)(2,1)S(1)}, bf16[2048,4]{0,1:T(4,128)(2,1)}, u32[]{:S(2)}) copy-start(bf16[2048,4]{0,1:T(4,128)(2,1)} %param.34) | copy-start | bytes 49156
  19.2 18.0 %collective-permute-start.1 = (bf16[2,512,128]{2,1,0:T(8,128)(2,1)S(1)}, bf16[2,512,128]{2,1,0:T(8,128)(2,1)S(1)}, u32[]{:S(2)}, u32[]{:S(2)}) collective-permute-start(bf16[2,512,128]{2,1,0:T(8,128)(2,1)S(1)} %pad_maximum_fusion.near), channel_id=1, source_target_pairs={{0,2},{1,3},{2,0},{3,1},{4,6},{5,7},{6,4},{7,5},{8,10},{9,11},{10,... | collective-permute-start | bytes 786440 | tf_op jit(solution)/shard_map/cross/ppermute | solution.py:170
  26.1 22.0 %copy-start.3 = (bf16[1,2048,128]{2,1,0:T(8,128)(2,1)S(1)}, bf16[1,2048,128]{2,1,0:T(8,128)(2,1)}, u32[]{:S(2)}) copy-start(bf16[1,2048,128]{2,1,0:T(8,128)(2,1)} %w_up.1) | copy-start | bytes 1572868
  26.1 22.0 %copy-start.4 = (bf16[1,128,2048]{2,1,0:T(8,128)(2,1)S(1)}, bf16[1,128,2048]{2,1,0:T(8,128)(2,1)}, u32[]{:S(2)}) copy-start(bf16[1,128,2048]{2,1,0:T(8,128)(2,1)} %w_down.1) | copy-start | bytes 1572868
  27.1 21.0 %copy-start.2 = (bf16[1,2048,128]{2,1,0:T(8,128)(2,1)S(1)}, bf16[1,2048,128]{2,1,0:T(8,128)(2,1)}, u32[]{:S(2)}) copy-start(bf16[1,2048,128]{2,1,0:T(8,128)(2,1)} %w_gate.1) | copy-start | bytes 1572868
  27.1 10.1 %all-to-all-start.2 = ((bf16[32,2,512]{2,1,0:T(2,128)(2,1)}), bf16[32,2,512]{2,1,0:T(2,128)(2,1)S(1)}, u32[]{:S(2)}, u32[]{:S(2)}) async-start(bf16[32,2,512]{2,1,0:T(2,128)(2,1)} %get-tuple-element.10), calls=%async_computation.2 | async-start | bytes 131072 | tf_op jit(solution)/shard_map/r3/all_to_all | solution.py:17
  38.1 10.0 %all-to-all-start.3 = ((bf16[32,8,128]{2,1,0:T(8,128)(2,1)}), bf16[32,8,128]{2,1,0:T(8,128)(2,1)S(1)}, u32[]{:S(2)}, u32[]{:S(2)}) async-start(bf16[32,8,128]{2,1,0:T(8,128)(2,1)} %output.1), calls=%async_computation.3 | async-start | bytes 131072 | tf_op jit(solution)/shard_map/r4/all_to_all | solution.py:17
  40.6 7.4 %copy-start.10 = (f32[2048]{0:T(1024)S(1)}, f32[2048]{0:T(1024)}, u32[]{:S(2)}) copy-start(f32[2048]{0:T(1024)} %param.33) | copy-start | bytes 24580
  49.9 10.0 %all-to-all-start.4 = ((bf16[32,2,512]{2,1,0:T(2,128)(2,1)}), bf16[32,2,512]{2,1,0:T(2,128)(2,1)S(1)}, u32[]{:S(2)}, u32[]{:S(2)}) async-start(bf16[32,2,512]{2,1,0:T(2,128)(2,1)} %get-tuple-element.13), calls=%async_computation.4 | async-start | bytes 131072 | tf_op jit(solution)/shard_map/r5/all_to_all | solution.py:17
  (4 other events, 2.6 us)
